TPU v7x, 32 devices: a whole 2x2x4 slice. The times are simulated.
32 devices in a mesh: ep: 8 (over z, x), tp: 4 (over y, core).
Axes of the slice: x: 2, y: 2, z: 4, core: 2. Of those that a mesh axis runs over, the one named last changes fastest.
Arguments:
- queries: bfloat16 [2048, 1536], P('ep', 'tp'), may hold values from -600 to 600
- compressed_key_value: bfloat16 [2048, 512], P('ep'), may hold values from -6 to 6
- rope_key: bfloat16 [2048, 32], P('ep'), may hold values from -6 to 6
- latent_norm_gain: float32 [512], replicated, may hold values from 0.1 to 1.9
- latent_to_key_value: bfloat16 [512, 2048], P(None, 'tp'), may hold values from -0.25 to 0.25
- out_proj: bfloat16 [1024, 2048], P(None, 'tp'), may hold values from -1.5 to 1.5
- moe_input: bfloat16 [2048, 2048], P('ep'), may hold values from -6 to 6
- moe_gain: float32 [2048], replicated, may hold values from 0.1 to 1.9
- routes: int32 [2048, 2], P('ep'), may hold values from 0 to 7, all different within a row; in each aligned block of 256 rows (0 to 255, 256 to 511, ...) at most 96 rows name the same one
- route_weight: float32 [2048, 2], P('ep'), may hold values from 0.2 to 1
- gate_weight: bfloat16 [8, 2048, 4096], P('ep', None, 'tp'), may hold values from -0.125 to 0.125
- up_weight: bfloat16 [8, 2048, 4096], P('ep', None, 'tp'), may hold values from -0.125 to 0.125
- down_weight: bfloat16 [8, 4096, 2048], P('ep', 'tp'), may hold values from -0.09375 to 0.09375
Outputs:
- attention_out: bfloat16 [2048, 2048], P('ep', 'tp')
- expert_out: bfloat16 [2048, 2048], P('ep', 'tp')
Inputs may be any that keep to these rules, and one draw needn't show every extreme that they name: `routes`: each row names 2 different experts. In the rows of one device (aligned blocks of 256 rows) no expert is named by more than 96 rows, and in some blocks one expert is named by exactly 96 rows.
All inputs are finite; a program needn't handle non-finite values.
Results may differ from a plain program's by a relative error of at most 0.019.
The roundings to bfloat16 on the way count: a program that leaves them out, or rounds other values in their place, can miss the bound.
Values may be sent and summed in bfloat16 or wider, within the bound.
A program may use at most 128 MiB of HBM per device.

v0:
```python
import math
import jax
import jax.numpy as jnp
from jax import lax
from jax.sharding import PartitionSpec as P

PLAIN_HEAD_DIM = 64
ROPE = 32
VALUE_HEAD_DIM = 64
EPSILON = 1e-06
ROPE_BASE_VALUE = 10000.0


def rms_scale(values, gain_vector):
    floats = values.astype(jnp.float32)
    return (
        floats
        * lax.rsqrt(jnp.mean(floats * floats, axis=-1, keepdims=True) + EPSILON)
        * gain_vector
    )


def rotary(values, positions):
    full_width = values.shape[-1]
    half_dim = full_width // 2
    frequency = ROPE_BASE_VALUE ** (-jnp.arange(half_dim, dtype=jnp.float32) * 2.0 / full_width)
    angles = positions[..., None] * frequency
    cosine = jnp.cos(angles)
    sine_part = jnp.sin(angles)
    first_half = values[..., :half_dim]
    second_half = values[..., half_dim:]
    return jnp.concatenate(
        [
            first_half * cosine - second_half * sine_part,
            second_half * cosine + first_half * sine_part,
        ],
        axis=-1,
    )


def slot_table(block_routes, capacity, experts):
    flat_routes = block_routes.reshape(-1)
    onehot_table = (flat_routes[:, None] == jnp.arange(experts, dtype=jnp.int32)[None, :]).astype(
        jnp.int32
    )
    earlier = jnp.cumsum(onehot_table, axis=0) - onehot_table
    slot_index = jnp.sum(earlier * onehot_table, axis=1)
    destination = flat_routes * capacity + slot_index
    token_count = block_routes.shape[0]
    source_rows = jnp.arange(flat_routes.shape[0], dtype=jnp.int32) // block_routes.shape[1]
    source_table = (
        jnp.full((experts * capacity,), token_count, jnp.int32).at[destination].set(source_rows)
    )
    return (destination, source_table)


def local(
    queries,
    compressed_key_value,
    rope_key,
    latent_norm_gain,
    latent_to_key_value,
    out_proj,
    moe_input,
    moe_gain,
    routes,
    route_weight,
    gate_weight,
    up_weight,
    down_weight,
):
    row_count = queries.shape[0]
    head_count = latent_to_key_value.shape[1] // (PLAIN_HEAD_DIM + VALUE_HEAD_DIM)
    offset = lax.axis_index("ep") * row_count
    positions = (offset + jnp.arange(row_count, dtype=jnp.int32)).astype(jnp.float32)
    query_heads = queries.reshape(row_count, head_count, PLAIN_HEAD_DIM + ROPE)
    query_nope = query_heads[..., :PLAIN_HEAD_DIM]
    query_rope = rotary(
        query_heads[..., PLAIN_HEAD_DIM:].astype(jnp.float32), positions[:, None]
    ).astype(jnp.bfloat16)
    latent_normed = rms_scale(compressed_key_value, latent_norm_gain).astype(jnp.bfloat16)
    key_rope = rotary(rope_key.astype(jnp.float32), positions).astype(jnp.bfloat16)
    score_scale = (PLAIN_HEAD_DIM + ROPE) ** (-0.5)

    def attend_block(state_now, key_value, block_rope):
        run_max, run_total, run_values = state_now
        key_nope = key_value[..., :PLAIN_HEAD_DIM]
        block_values = key_value[..., PLAIN_HEAD_DIM:]
        scores = (
            jnp.einsum("qhd,khd->qhk", query_nope, key_nope, preferred_element_type=jnp.float32)
            + jnp.einsum("qhr,kr->qhk", query_rope, block_rope, preferred_element_type=jnp.float32)
        ) * score_scale
        new_max = jnp.maximum(run_max, jnp.max(scores, axis=-1))
        shrink = jnp.exp(run_max - new_max)
        weights = jnp.exp(scores - new_max[..., None])
        run_total = run_total * shrink + jnp.sum(weights, axis=-1)
        run_values = run_values * shrink[..., None] + jnp.einsum(
            "qhk,khd->qhd",
            weights.astype(jnp.bfloat16),
            block_values,
            preferred_element_type=jnp.float32,
        )
        return (new_max, run_total, run_values)

    initial = (
        jnp.full((row_count, head_count), -jnp.inf, jnp.float32),
        jnp.zeros((row_count, head_count), jnp.float32),
        jnp.zeros((row_count, head_count, VALUE_HEAD_DIM), jnp.float32),
    )

    def expand_latent(block_main):
        own_heads = jnp.dot(
            block_main, latent_to_key_value, preferred_element_type=jnp.float32
        ).astype(jnp.bfloat16)
        return own_heads.reshape(block_main.shape[0], head_count, PLAIN_HEAD_DIM + VALUE_HEAD_DIM)

    piece_main = lax.all_gather(latent_normed, "ep", axis=0, tiled=True)
    piece_rope = lax.all_gather(key_rope, "ep", axis=0, tiled=True)
    piece_rows = piece_main.shape[0]
    group_rows = math.gcd(piece_rows, 2048)
    block_count = piece_rows // group_rows
    main_blocks = piece_main.reshape(block_count, group_rows, piece_main.shape[1])
    rope_blocks = piece_rope.reshape(block_count, group_rows, piece_rope.shape[1])

    def step_block(state_inner, block_data):
        block_main, block_rope = block_data
        return (attend_block(state_inner, expand_latent(block_main), block_rope), None)

    state_out, unused = lax.scan(step_block, initial, (main_blocks, rope_blocks))
    run_max, run_total, run_values = state_out
    attended = (
        (run_values / run_total[..., None])
        .astype(jnp.bfloat16)
        .reshape(row_count, head_count * VALUE_HEAD_DIM)
    )
    projected = jnp.dot(
        lax.all_gather(attended, "tp", axis=1, tiled=True),
        out_proj,
        preferred_element_type=jnp.float32,
    )
    attention_out = projected.astype(jnp.bfloat16)
    moe_rows = moe_input.shape[0]
    model_width = moe_input.shape[1]
    expert_local = gate_weight.shape[0]
    ep_count = lax.axis_size("ep")
    tp_count = lax.axis_size("tp")
    expert_total = ep_count * expert_local
    capacity = 3 * moe_rows // ep_count
    normed = rms_scale(moe_input, moe_gain).astype(jnp.bfloat16)
    destination, source_table = slot_table(routes, capacity, expert_total)
    padded = jnp.concatenate([normed, jnp.zeros((1, model_width), jnp.bfloat16)], axis=0)
    outgoing = padded[source_table].reshape(ep_count, expert_local, capacity, model_width)
    column_width = model_width // tp_count
    own_columns = lax.dynamic_slice_in_dim(
        outgoing, lax.axis_index("tp") * column_width, column_width, 3
    )
    arrived_whole = lax.all_gather(
        lax.all_to_all(own_columns, "ep", split_axis=0, concat_axis=0, tiled=True),
        "tp",
        axis=3,
        tiled=True,
    )
    gate_value = jnp.einsum(
        "sexd,edf->sexf", arrived_whole, gate_weight, preferred_element_type=jnp.float32
    )
    up_value = jnp.einsum(
        "sexd,edf->sexf", arrived_whole, up_weight, preferred_element_type=jnp.float32
    )
    hidden = (jax.nn.silu(gate_value) * up_value).astype(jnp.bfloat16)
    partial_out = jnp.einsum(
        "sexf,efd->sexd", hidden, down_weight, preferred_element_type=jnp.float32
    )
    summed = lax.psum_scatter(
        partial_out.astype(jnp.bfloat16), "tp", scatter_dimension=3, tiled=True
    )
    returned = lax.all_to_all(summed, "ep", split_axis=0, concat_axis=0, tiled=True)
    flat_back = returned.reshape(expert_total * capacity, returned.shape[3])
    picked = (
        flat_back[destination]
        .astype(jnp.float32)
        .reshape(moe_rows, routes.shape[1], returned.shape[3])
    )
    expert_out = jnp.sum(picked * route_weight[..., None], axis=1).astype(jnp.bfloat16)
    return (attention_out, expert_out)


def solution(mesh):
    return jax.shard_map(
        local,
        mesh=mesh,
        in_specs=(
            P("ep", "tp"),
            P("ep", None),
            P("ep", None),
            P(),
            P(None, "tp"),
            P(None, "tp"),
            P("ep", None),
            P(),
            P("ep", None),
            P("ep", None),
            P("ep", None, "tp"),
            P("ep", None, "tp"),
            P("ep", "tp", None),
        ),
        out_specs=(P("ep", "tp"), P("ep", "tp")),
        check_vma=False,
    )
```

profile of v0, /device:TPU:0, one launch (start us, length us, event | category | flops | bytes accessed | tf_op | source)
XLA Modules:
  0.0 206.0 jit_solution(7960402563540832148)
XLA Ops:
  9.1 1.1 reduce-window.6
  10.9 2.4 %scatter_custom_fusion = s32[768]{0:T(1024)S(1)} fusion(s32[512]{0:T(512)S(1)} %bitcast.124, s32[512]{0:T(512)S(1)} %add_select_fusion, s32[]{:T(128)} %constant.45.clone.1), kind=kCustom, calls=%fused_computation.79 | custom fusion | bytes 3076 | tf_op jit(solution)/shard_map/scatter | solution.py:52
  13.4 1.5 fusion.24
  14.9 1.5 fusion.26
  16.5 4.3 %gather_fusion = bf16[768,2048]{1,0:T(8,128)(2,1)} fusion(bf16[257,2048]{1,0:T(8,128)(2,1)S(1)} %concatenate.13, s32[1024]{0:T(1024)S(1)} %pad_clamp_fusion.1), kind=kCustom, calls=%fused_computation | custom fusion | bytes 6294528 | tf_op jit(solution)/shard_map/gather | solution.py:152
  20.8 1.2 constant_dynamic-slice_fusion
  22.0 27.3 %all_to_all.10 = bf16[8,1,96,512]{3,2,1,0:T(8,128)(2,1)} all-to-all(bf16[8,1,96,512]{3,2,1,0:T(8,128)(2,1)S(1)} %constant_dynamic-slice_fusion), channel_id=1, replica_groups=mesh['ep'=8,'tp'=4] {'ep'}, dimensions={0} | all-to-all | bytes 1572864 | tf_op jit(solution)/shard_map/all_to_all | solution.py:158
  50.5 26.6 %all-gather.5.cloned.1.call-done = bf16[8,1,96,2048]{3,2,0,1:T(8,128)(2,1)} async-done(((bf16[8,1,96,512]{3,2,0,1:T(8,128)(2,1)}), bf16[8,1,96,2048]{3,2,0,1:T(8,128)(2,1)}) %all-gather.5.cloned.1.call-update) | async-done | bytes 3145744 | tf_op jit(solution)/shard_map/all_gather | solution.py:157
  77.1 8.3 %fusion.7 = f32[8,96,1024]{2,1,0:T(8,128)} fusion(bf16[1,2048,1024]{2,1,0:T(8,128)(2,1)} %param.24, bf16[8,1,96,2048]{3,2,0,1:T(8,128)(2,1)} %all-gather.5.cloned.1.call-done), kind=kOutput, calls=%fused_computation.11 | convolution fusion | flops 3221225472 | bytes 10485760 | tf_op jit(solution)/shard_map/sexd,edf->sexf/dot_general | solution.py:166
  85.4 12.9 %fusion.21 = bf16[8,1,96,2048]{3,2,0,1:T(8,128)(2,1)} fusion(bf16[1,1024,2048]{2,1,0:T(8,128)(2,1)} %param.25, f32[8,96,1024]{2,1,0:T(8,128)} %fusion.7, bf16[1,2048,1024]{2,1,0:T(8,128)(2,1)} %param.23, bf16[8,1,96,2048]{3,2,0,1:T(8,128)(2,1)} %all-gather.5.cloned.1.call-done), kind=kOutput, calls=%fused_computation.26 | convolution fusion | flops 6448742400 | bytes 17825792 | tf_op jit(solution)/shard_map/sexf,efd->sexd/dot_general | solution.py:170
  99.7 31.5 %all_gather.13 = bf16[2048,32]{0,1:T(8,128)(2,1)S(1)} all-gather(bf16[256,32]{0,1:T(8,128)(2,1)S(1)} %pad_maximum_fusion), channel_id=1, replica_groups=mesh['ep'=8,'tp'=4] {'ep'}, dimensions={0}, use_global_device_ids=true | all-gather | bytes 147456 | tf_op jit(solution)/shard_map/all_gather | solution.py:118
  131.3 2.9 %convolution_convert_fusion = bf16[2048,512]{0,1:T(8,128)(2,1)S(1)} fusion(bf16[2048,512]{1,0:T(8,128)(2,1)} %all-gather.3.cloned.1.call-done, bf16[512,512]{1,0:T(8,128)(2,1)S(1)} %copy-done.8), kind=kOutput, calls=%fused_computation.27 | convolution fusion | flops 1074790400 | bytes 4718592 | tf_op jit(solution)/shard_map/while/body/eval_jaxpr/dot_general | solution.py:112
  134.2 1.3 fusion.53
  135.6 5.0 %fusion.74 = (f32[256,4]{0,1:T(4,128)S(1)}, f32[256,4,2048]{0,2,1:T(8,128)}) fusion(bf16[2048,32]{0,1:T(8,128)(2,1)S(1)} %all_gather.13, bf16[256,4,16]{0,2,1:T(8,128)(2,1)S(1)} %get-tuple-element.21, bf16[256,4,16]{0,2,1:T(8,128)(2,1)S(1)} %get-tuple-element.20, f32[4,2048,256]{2,1,0:T(8,128)S(1)} %fusion.53), kind=kOutput, calls=%fused_computation.91 | convolution fusion | flops 140639232 | bytes 16977920 | tf_op jit(solution)/shard_map/while/body/eval_jaxpr/qhr,kr->qhk/dot_general | solution.py:91
  140.6 28.6 %reduce-scatter.2.cloned.1.call-done = bf16[8,1,96,512]{3,2,0,1:T(8,128)(2,1)} async-done(((bf16[8,1,96,2048]{3,2,0,1:T(8,128)(2,1)}), bf16[8,1,96,512]{3,2,0,1:T(8,128)(2,1)}) %reduce-scatter.2.cloned.1.call-update) | async-done | bytes 786448 | tf_op jit(solution)/shard_map/reduce_scatter | solution.py:173
  169.2 5.5 %all-to-all-start.1 = ((bf16[8,1,96,512]{3,2,1,0:T(8,128)(2,1)}), bf16[8,1,96,512]{3,2,1,0:T(8,128)(2,1)S(1)}, u32[]{:S(2)}, u32[]{:S(2)}) async-start(bf16[8,1,96,512]{3,2,1,0:T(8,128)(2,1)} %bitcast.122), calls=%async_computation.2 | async-start | bytes 1572864 | tf_op jit(solution)/shard_map/all_to_all | solution.py:176
  174.7 4.6 %fusion.1 = f32[256,4]{0,1:T(4,128)S(1)} fusion(f32[256,4,2048]{0,2,1:T(8,128)} %get-tuple-element.40, f32[256,4]{0,1:T(4,128)S(1)} %get-tuple-element.39), kind=kLoop, calls=%fused_computation.6 | loop fusion | flops 4193280 | bytes 8396800 | tf_op jit(solution)/shard_map/while/body/eval_jaxpr/reduce_sum | solution.py:96
  179.4 1.1 copy-done.1
  180.5 2.7 %fusion.41 = bf16[256,4,64]{0,2,1:T(8,128)(2,1)S(1)} fusion(f32[256,4,2048]{0,2,1:T(8,128)S(1)} %copy-done.1, f32[256,4]{0,1:T(4,128)S(1)} %get-tuple-element.39, bf16[2048,4,128]{0,2,1:T(8,128)(2,1)} %bitcast.119, f32[256,4]{0,1:T(4,128)S(1)} %get-tuple-element.25, f32[256,4]{0,1:T(4,128)S(1)} %get-tuple-element.24), kind=kOutput, calls=%fused_computation.38 | convolution fusion | flops 272826368 | bytes 9580544 | tf_op jit(solution)/shard_map/while/body/eval_jaxpr/qhk,khd->qhd/dot_general | solution.py:97
  183.1 6.5 %all_gather.14 = bf16[256,1024]{0,1:T(8,128)(2,1)S(1)} all-gather(bf16[256,256]{0,1:T(8,128)(2,1)S(1)} %bitcast.123), channel_id=1, replica_groups=mesh['ep'=8,'tp'=4] {'tp'}, dimensions={1}, use_global_device_ids=true | all-gather | bytes 655360 | tf_op jit(solution)/shard_map/all_gather | solution.py:137
  189.6 1.2 convolution_convert_fusion.1
  190.8 4.0 %all-to-all-done.1 = bf16[8,1,96,512]{3,2,1,0:T(8,128)(2,1)S(1)} async-done(((bf16[8,1,96,512]{3,2,1,0:T(8,128)(2,1)}), bf16[8,1,96,512]{3,2,1,0:T(8,128)(2,1)S(1)}, u32[]{:S(2)}, u32[]{:S(2)}) %all-to-all-start.1) | async-done | bytes 786464 | tf_op jit(solution)/shard_map/all_to_all | solution.py:176
  194.8 2.0 gather_fusion.1
  197.4 2.1 multiply_reduce_fusion
  (56 shorter events, 5.9 us)
Async XLA Ops:
  7.2 182.5 %copy-start = (bf16[1024,512]{1,0:T(8,128)(2,1)S(1)}, bf16[1024,512]{1,0:T(8,128)(2,1)}, u32[]{:S(2)}) copy-start(bf16[1024,512]{1,0:T(8,128)(2,1)} %param.18) | copy-start | bytes 3145732
  7.2 69.9 %all-gather.5.cloned.1.call-start = ((), (), s32[]{:S(2)}) async-start(), calls=%async_computation.4 | async-start | bytes 3932160 | tf_op jit(solution)/shard_map/all_gather | solution.py:157
  20.8 28.6 %copy-start.3 = (bf16[256,512]{1,0:T(8,128)(2,1)S(1)}, bf16[256,512]{1,0:T(8,128)(2,1)}, u32[]{:S(2)}) copy-start(bf16[256,512]{1,0:T(8,128)(2,1)} %param.14) | copy-start | bytes 786436
  20.8 28.8 %copy-start.6 = (f32[512]{0:T(512)S(1)}, f32[512]{0:T(512)}, u32[]{:S(2)}) copy-start(f32[512]{0:T(512)} %param.16) | copy-start | bytes 6148
  49.4 81.8 %all-gather.3.cloned.1.call-start = ((), (), s32[]{:S(2)}) async-start(), calls=%async_computation.3 | async-start | bytes 2359296 | tf_op jit(solution)/shard_map/all_gather | solution.py:117
  50.5 118.7 %reduce-scatter.2.cloned.1.call-start = ((), (), s32[]{:S(2)}) async-start(), calls=%async_computation.5 | async-start | bytes 3932160 | tf_op jit(solution)/shard_map/reduce_scatter | solution.py:173
  98.2 0.7 copy-start.5
  98.2 0.9 copy-start.4
  98.2 1.1 copy-start.7
  98.2 33.0 %copy-start.8 = (bf16[512,512]{1,0:T(8,128)(2,1)S(1)}, bf16[512,512]{1,0:T(8,128)(2,1)}, u32[]{:S(2)}) copy-start(bf16[512,512]{1,0:T(8,128)(2,1)} %param.17) | copy-start | bytes 1572868
  134.2 1.4 copy-start.2
  169.2 25.6 %all-to-all-start.1 = ((bf16[8,1,96,512]{3,2,1,0:T(8,128)(2,1)}), bf16[8,1,96,512]{3,2,1,0:T(8,128)(2,1)S(1)}, u32[]{:S(2)}, u32[]{:S(2)}) async-start(bf16[8,1,96,512]{3,2,1,0:T(8,128)(2,1)} %bitcast.122), calls=%async_computation.2 | async-start | bytes 1572864 | tf_op jit(solution)/shard_map/all_to_all | solution.py:176
  174.7 5.8 %copy-start.1 = (f32[256,4,2048]{0,2,1:T(8,128)S(1)}, f32[256,4,2048]{0,2,1:T(8,128)}, u32[]{:S(2)}) copy-start(f32[256,4,2048]{0,2,1:T(8,128)} %get-tuple-element.40) | copy-start | bytes 25165828
Sparse Core Ops, SparseCore 0:
  49.5 27.5 all-gather.4
  79.8 50.4 all-gather.2
  132.8 36.3 reduce-scatter.1
where the time goes:
time: 206 us
  blocking collectives  65.3 us (32%)
  waiting for transfers between devices  59.3 us (29%)
  matrix products  34.2 us (17%)
  local copies, waits for them, and re-layouts  14.7 us (7%)
  between operations  14 us (7%)
  other arithmetic  12.9 us (6%)
  starting transfers between devices  5.61 us (3%)
    all_gather x1, blocking collectives, local(): piece_rope = lax.all_gather(key_rope, 'ep', axis=0, tiled=True)  31.5 us
    reduce_scatter x1, waiting for transfers between devices, local(): lax.psum_scatter(partial_out.astype(jnp.bfloat16), 'tp', scatter_dimensio...  28.6 us
    all_to_all x1, blocking collectives, local(): lax.all_to_all(own_columns, 'ep', split_axis=0, concat_axis=0, tiled=True)  27.3 us
    all_gather x1, waiting for transfers between devices, local(): lax.all_gather(lax.all_to_all(own_columns, 'ep', split_axis=0, concat_axi...  26.6 us
    dot_general x1, matrix products, local(): jnp.einsum('sexf,efd->sexd', hidden, down_weight, preferred_element_type=...  12.9 us
    dot_general x1, matrix products, local(): jnp.einsum('sexd,edf->sexf', arrived_whole, up_weight, preferred_element_...  8.26 us
    all_gather x1, blocking collectives, local(): lax.all_gather(attended, 'tp', axis=1, tiled=True)  6.5 us
    all_to_all x1, starting transfers between devices, local(): lax.all_to_all(summed, 'ep', split_axis=0, concat_axis=0, tiled=True)  5.49 us
  transfers between devices with their start and end apart: 4, of which 3 were waited for; matrix products, arithmetic and copies ran while one was open for 20% of the time, Pallas kernels for 0%

commit v1 on v0

--- a/solution.py
+++ b/solution.py
@@ -114,8 +114,13 @@
         ).astype(jnp.bfloat16)
         return own_heads.reshape(block_main.shape[0], head_count, PLAIN_HEAD_DIM + VALUE_HEAD_DIM)
 
-    piece_main = lax.all_gather(latent_normed, "ep", axis=0, tiled=True)
-    piece_rope = lax.all_gather(key_rope, "ep", axis=0, tiled=True)
+    piece_main, piece_rope = jnp.split(
+        lax.all_gather(
+            jnp.concatenate([latent_normed, key_rope], axis=1), "ep", axis=0, tiled=True
+        ),
+        [latent_normed.shape[1]],
+        axis=1,
+    )
     piece_rows = piece_main.shape[0]
     group_rows = math.gcd(piece_rows, 2048)
     block_count = piece_rows // group_rows

time: 206 us -> 207 us (level)
  blocking collectives: 65.3 us -> 34 us
  waiting for transfers between devices: 59.3 us -> 89.7 us
    all_gather x1, waiting for transfers between devices: 0.02 us -> 31.6 us  [local(): lax.all_gather(jnp.concatenate([latent_normed, key_rope], axis=1), 'ep',...]
    all_gather x1 -> x0, blocking collectives: 31.5 us -> none  [local(): piece_rope = lax.all_gather(key_rope, 'ep', axis=0, tiled=True)]
  transfers between devices with their start and end apart: 4 -> 4, of which waited for: 3 -> 4; matrix products, arithmetic and copies ran while one was open for 20% -> 20% of each run, Pallas kernels for 0% -> 0%
where the time goes in v1:
time: 207 us; the launch traced here: 206 us
  waiting for transfers between devices  89.7 us (43%)
  matrix products  35.1 us (17%)
  blocking collectives  34 us (16%)
  local copies, waits for them, and re-layouts  14.7 us (7%)
  between operations  14 us (7%)
  other arithmetic  13 us (6%)
  starting transfers between devices  5.81 us (3%)
    all_gather x1, waiting for transfers between devices, local(): lax.all_gather(jnp.concatenate([latent_normed, key_rope], axis=1), 'ep',...  31.6 us
    reduce_scatter x1, waiting for transfers between devices, local(): lax.psum_scatter(partial_out.astype(jnp.bfloat16), 'tp', scatter_dimensio...  28.3 us
    all_to_all x1, blocking collectives, local(): lax.all_to_all(own_columns, 'ep', split_axis=0, concat_axis=0, tiled=True)  27.3 us
    all_gather x1, waiting for transfers between devices, local(): lax.all_gather(lax.all_to_all(own_columns, 'ep', split_axis=0, concat_axi...  26 us
    dot_general x1, matrix products, local(): jnp.einsum('sexf,efd->sexd', hidden, down_weight, preferred_element_type=...  12.9 us
    dot_general x1, matrix products, local(): jnp.einsum('sexd,edf->sexf', arrived_whole, up_weight, preferred_element_...  8.26 us
    all_gather x1, blocking collectives, local(): lax.all_gather(attended, 'tp', axis=1, tiled=True)  6.72 us
    dot_general x1, matrix products, attend_block(): jnp.einsum('qhr,kr->qhk', query_rope, block_rope, preferred_element_type=...  5.97 us
  transfers between devices with their start and end apart: 4, of which 4 were waited for; matrix products, arithmetic and copies ran while one was open for 20% of the time, Pallas kernels for 0%

profile of v1, /device:TPU:0, one launch (start us, length us, event | category | flops | bytes accessed | tf_op | source)
XLA Modules:
  0.0 206.4 jit_solution(13474929195461434114)
XLA Ops:
  9.1 1.5 fusion.24
  10.9 1.1 reduce-window.6
  12.4 2.4 %scatter_custom_fusion = s32[768]{0:T(1024)S(1)} fusion(s32[512]{0:T(512)S(1)} %bitcast.123, s32[512]{0:T(512)S(1)} %add_select_fusion, s32[]{:T(128)} %constant.45.clone.1), kind=kCustom, calls=%fused_computation.80 | custom fusion | bytes 3076 | tf_op jit(solution)/shard_map/scatter | solution.py:52
  14.9 1.5 fusion.26
  16.6 4.3 %gather_fusion = bf16[768,2048]{1,0:T(8,128)(2,1)} fusion(bf16[257,2048]{1,0:T(8,128)(2,1)S(1)} %concatenate.15, s32[1024]{0:T(1024)S(1)} %pad_clamp_fusion.1), kind=kCustom, calls=%fused_computation | custom fusion | bytes 6294528 | tf_op jit(solution)/shard_map/gather | solution.py:157
  20.8 1.2 constant_dynamic-slice_fusion
  22.1 27.3 %all_to_all.10 = bf16[8,1,96,512]{3,2,1,0:T(8,128)(2,1)} all-to-all(bf16[8,1,96,512]{3,2,1,0:T(8,128)(2,1)S(1)} %constant_dynamic-slice_fusion), channel_id=1, replica_groups=mesh['ep'=8,'tp'=4] {'ep'}, dimensions={0} | all-to-all | bytes 1572864 | tf_op jit(solution)/shard_map/all_to_all | solution.py:163
  51.1 26.0 %all-gather.5.cloned.1.call-done = bf16[8,1,96,2048]{3,2,0,1:T(8,128)(2,1)} async-done(((bf16[8,1,96,512]{3,2,0,1:T(8,128)(2,1)}), bf16[8,1,96,2048]{3,2,0,1:T(8,128)(2,1)}) %all-gather.5.cloned.1.call-update) | async-done | bytes 3145744 | tf_op jit(solution)/shard_map/all_gather | solution.py:162
  77.1 8.3 %fusion.7 = f32[8,96,1024]{2,1,0:T(8,128)} fusion(bf16[1,2048,1024]{2,1,0:T(8,128)(2,1)} %param.24, bf16[8,1,96,2048]{3,2,0,1:T(8,128)(2,1)} %all-gather.5.cloned.1.call-done), kind=kOutput, calls=%fused_computation.11 | convolution fusion | flops 3221225472 | bytes 10485760 | tf_op jit(solution)/shard_map/sexd,edf->sexf/dot_general | solution.py:171
  85.4 12.9 %fusion.21 = bf16[8,1,96,2048]{3,2,0,1:T(8,128)(2,1)} fusion(bf16[1,1024,2048]{2,1,0:T(8,128)(2,1)} %param.25, f32[8,96,1024]{2,1,0:T(8,128)} %fusion.7, bf16[1,2048,1024]{2,1,0:T(8,128)(2,1)} %param.23, bf16[8,1,96,2048]{3,2,0,1:T(8,128)(2,1)} %all-gather.5.cloned.1.call-done), kind=kOutput, calls=%fused_computation.26 | convolution fusion | flops 6448742400 | bytes 17825792 | tf_op jit(solution)/shard_map/sexf,efd->sexd/dot_general | solution.py:175
  99.5 31.6 %all-gather.3.cloned.1.call-done = bf16[2048,544]{0,1:T(8,128)(2,1)} async-done(((bf16[256,544]{0,1:T(8,128)(2,1)}), bf16[2048,544]{0,1:T(8,128)(2,1)}) %all-gather.3.cloned.1.call-update) | async-done | bytes 2228240 | tf_op jit(solution)/shard_map/all_gather | solution.py:118
  131.1 2.9 %convolution_convert_fusion = bf16[2048,512]{0,1:T(8,128)(2,1)S(1)} fusion(bf16[512,512]{1,0:T(8,128)(2,1)S(1)} %copy-done.8, bf16[2048,544]{0,1:T(8,128)(2,1)} %all-gather.3.cloned.1.call-done), kind=kOutput, calls=%fused_computation.27 | convolution fusion | flops 1074790400 | bytes 4718592 | tf_op jit(solution)/shard_map/while/body/eval_jaxpr/dot_general | solution.py:112
  134.0 1.3 fusion.54
  135.3 6.0 %fusion.74 = (f32[256,4]{0,1:T(4,128)S(1)}, f32[256,4,2048]{0,2,1:T(8,128)}) fusion(bf16[2048,544]{0,1:T(8,128)(2,1)} %all-gather.3.cloned.1.call-done, bf16[256,4,16]{0,2,1:T(8,128)(2,1)S(1)} %get-tuple-element.21, bf16[256,4,16]{0,2,1:T(8,128)(2,1)S(1)} %get-tuple-element.20, f32[4,2048,256]{2,1,0:T(8,128)S(1)} %fusion.54), kind=kOutput, calls=%fused_computation.92 | convolution fusion | flops 140639232 | bytes 16977920 | tf_op jit(solution)/shard_map/while/body/eval_jaxpr/qhr,kr->qhk/dot_general | solution.py:91
  141.3 28.3 %reduce-scatter.2.cloned.1.call-done = bf16[8,1,96,512]{3,2,0,1:T(8,128)(2,1)} async-done(((bf16[8,1,96,2048]{3,2,0,1:T(8,128)(2,1)}), bf16[8,1,96,512]{3,2,0,1:T(8,128)(2,1)}) %reduce-scatter.2.cloned.1.call-update) | async-done | bytes 786448 | tf_op jit(solution)/shard_map/reduce_scatter | solution.py:178
  169.6 5.5 %all-to-all-start.1 = ((bf16[8,1,96,512]{3,2,1,0:T(8,128)(2,1)}), bf16[8,1,96,512]{3,2,1,0:T(8,128)(2,1)S(1)}, u32[]{:S(2)}, u32[]{:S(2)}) async-start(bf16[8,1,96,512]{3,2,1,0:T(8,128)(2,1)} %bitcast.121), calls=%async_computation.2 | async-start | bytes 1572864 | tf_op jit(solution)/shard_map/all_to_all | solution.py:181
  175.1 4.6 %fusion.1 = f32[256,4]{0,1:T(4,128)S(1)} fusion(f32[256,4,2048]{0,2,1:T(8,128)} %get-tuple-element.40, f32[256,4]{0,1:T(4,128)S(1)} %get-tuple-element.39), kind=kLoop, calls=%fused_computation.6 | loop fusion | flops 4193280 | bytes 8396800 | tf_op jit(solution)/shard_map/while/body/eval_jaxpr/reduce_sum | solution.py:96
  179.8 1.1 copy-done.1
  180.9 2.7 %fusion.42 = bf16[256,4,64]{0,2,1:T(8,128)(2,1)S(1)} fusion(f32[256,4,2048]{0,2,1:T(8,128)S(1)} %copy-done.1, f32[256,4]{0,1:T(4,128)S(1)} %get-tuple-element.39, bf16[2048,4,128]{0,2,1:T(8,128)(2,1)} %bitcast.118, f32[256,4]{0,1:T(4,128)S(1)} %get-tuple-element.25, f32[256,4]{0,1:T(4,128)S(1)} %get-tuple-element.24), kind=kOutput, calls=%fused_computation.39 | convolution fusion | flops 272826368 | bytes 9580544 | tf_op jit(solution)/shard_map/while/body/eval_jaxpr/qhk,khd->qhd/dot_general | solution.py:97
  183.6 6.7 %all_gather.10 = bf16[256,1024]{0,1:T(8,128)(2,1)S(1)} all-gather(bf16[256,256]{0,1:T(8,128)(2,1)S(1)} %bitcast.122), channel_id=1, replica_groups=mesh['ep'=8,'tp'=4] {'tp'}, dimensions={1}, use_global_device_ids=true | all-gather | bytes 655360 | tf_op jit(solution)/shard_map/all_gather | solution.py:142
  190.3 1.2 convolution_convert_fusion.1
  191.4 3.7 %all-to-all-done.1 = bf16[8,1,96,512]{3,2,1,0:T(8,128)(2,1)S(1)} async-done(((bf16[8,1,96,512]{3,2,1,0:T(8,128)(2,1)}), bf16[8,1,96,512]{3,2,1,0:T(8,128)(2,1)S(1)}, u32[]{:S(2)}, u32[]{:S(2)}) %all-to-all-start.1) | async-done | bytes 786464 | tf_op jit(solution)/shard_map/all_to_all | solution.py:181
  195.2 2.0 gather_fusion.1
  197.8 2.1 multiply_reduce_fusion
  (56 shorter events, 6.1 us)
Async XLA Ops:
  7.2 183.1 %copy-start = (bf16[1024,512]{1,0:T(8,128)(2,1)S(1)}, bf16[1024,512]{1,0:T(8,128)(2,1)}, u32[]{:S(2)}) copy-start(bf16[1024,512]{1,0:T(8,128)(2,1)} %param.18) | copy-start | bytes 3145732
  7.2 69.9 %all-gather.5.cloned.1.call-start = ((), (), s32[]{:S(2)}) async-start(), calls=%async_computation.4 | async-start | bytes 3932160 | tf_op jit(solution)/shard_map/all_gather | solution.py:162
  20.8 28.7 %copy-start.5 = (bf16[256,32]{0,1:T(8,128)(2,1)S(1)}, bf16[256,32]{0,1:T(8,128)(2,1)}, u32[]{:S(2)}) copy-start(bf16[256,32]{0,1:T(8,128)(2,1)} %param.15) | copy-start | bytes 49156
  20.8 28.7 %copy-start.3 = (bf16[256,512]{1,0:T(8,128)(2,1)S(1)}, bf16[256,512]{1,0:T(8,128)(2,1)}, u32[]{:S(2)}) copy-start(bf16[256,512]{1,0:T(8,128)(2,1)} %param.14) | copy-start | bytes 786436
  20.8 29.1 %copy-start.6 = (f32[512]{0:T(512)S(1)}, f32[512]{0:T(512)}, u32[]{:S(2)}) copy-start(f32[512]{0:T(512)} %param.16) | copy-start | bytes 6148
  49.4 81.7 %all-gather.3.cloned.1.call-start = ((), (), s32[]{:S(2)}) async-start(), calls=%async_computation.3 | async-start | bytes 2506752 | tf_op jit(solution)/shard_map/all_gather | solution.py:118
  50.9 118.8 %reduce-scatter.2.cloned.1.call-start = ((), (), s32[]{:S(2)}) async-start(), calls=%async_computation.5 | async-start | bytes 3932160 | tf_op jit(solution)/shard_map/reduce_scatter | solution.py:178
  98.2 0.9 copy-start.4
  98.2 1.1 copy-start.7
  98.2 32.9 %copy-start.8 = (bf16[512,512]{1,0:T(8,128)(2,1)S(1)}, bf16[512,512]{1,0:T(8,128)(2,1)}, u32[]{:S(2)}) copy-start(bf16[512,512]{1,0:T(8,128)(2,1)} %param.17) | copy-start | bytes 1572868
  134.0 1.3 copy-start.2
  169.6 25.6 %all-to-all-start.1 = ((bf16[8,1,96,512]{3,2,1,0:T(8,128)(2,1)}), bf16[8,1,96,512]{3,2,1,0:T(8,128)(2,1)S(1)}, u32[]{:S(2)}, u32[]{:S(2)}) async-start(bf16[8,1,96,512]{3,2,1,0:T(8,128)(2,1)} %bitcast.121), calls=%async_computation.2 | async-start | bytes 1572864 | tf_op jit(solution)/shard_map/all_to_all | solution.py:181
  175.1 5.8 %copy-start.1 = (f32[256,4,2048]{0,2,1:T(8,128)S(1)}, f32[256,4,2048]{0,2,1:T(8,128)}, u32[]{:S(2)}) copy-start(f32[256,4,2048]{0,2,1:T(8,128)} %get-tuple-element.40) | copy-start | bytes 25165828
Sparse Core Ops, SparseCore 0:
  49.5 27.5 all-gather.4
  79.2 51.8 all-gather.2
  133.6 35.9 reduce-scatter.1
